TPU v7x, 32 devices: a whole 2x2x4 slice. The times are simulated.
32 devices in a mesh: sp: 16 (over z, y, x), tp: 2 (over core).
Axes of the slice: x: 2, y: 2, z: 4, core: 2. Of those that a mesh axis runs over, the one named last changes fastest.
Arguments:
- queries: bfloat16 [4096, 8, 128], P('sp', 'tp'), may hold values from -6 to 6
- keys: bfloat16 [4096, 2, 128], P('sp'), may hold values from -6 to 6
- values: bfloat16 [4096, 2, 128], P('sp'), may hold values from -6 to 6
- documents: int32 [4096], P('sp'), may hold values from 0 to 3, never falling along the last dimension, each value on 1 to 2304 neighbouring positions
- query_gain: float32 [128], replicated, may hold values from 0.25 to 4
- key_gain: float32 [128], replicated, may hold values from 0.25 to 4
- out_weight: bfloat16 [1024, 2048], P('tp'), may hold values from -0.1875 to 0.1875
- residual: bfloat16 [4096, 2048], P('sp'), may hold values from -6 to 6
- norm_gain: float32 [2048], replicated, may hold values from 0.1 to 1.9
- up_weight: bfloat16 [2048, 6144], P('sp', 'tp'), may hold values from -0.125 to 0.125
- down_weight: bfloat16 [2048, 6144], P('sp', 'tp'), may hold values from -0.078125 to 0.078125
Outputs:
- layer_out: bfloat16 [4096, 2048], P(('sp', 'tp'))
Inputs may be any that keep to these rules, and one draw needn't show every extreme that they name: `documents`: document numbers never fall along the sequence; one document covers exactly (9) * 256 positions.
All inputs are finite; a program needn't handle non-finite values.
Results may differ from a plain program's by a relative error of at most 0.017.
Values may be sent and summed in bfloat16 or wider, within the bound.
A program may use at most 128 MiB of HBM per device.

v0:
```python
import jax
import jax.numpy as jnp
from jax import lax
from jax.sharding import PartitionSpec as P

QUERY_HEADS = 8
GRID = 64


EPS = 1e-06
THETA = 10000.0


def head_norm(block, gain):
    return block * lax.rsqrt(jnp.mean(block * block, axis=-1, keepdims=True) + EPS) * gain


def rotate(block, positions):
    head_width = block.shape[-1]
    pair_count = head_width // 4
    inverse = THETA ** (-jnp.arange(pair_count, dtype=jnp.float32) / pair_count)
    grid_row = (positions // GRID).astype(jnp.float32)[:, None] * inverse
    grid_col = (positions % GRID).astype(jnp.float32)[:, None] * inverse
    angles = jnp.concatenate([grid_row, grid_row, grid_col, grid_col], axis=-1)
    cosine = jnp.cos(angles)[:, None, :]
    sine_table = jnp.sin(angles)[:, None, :]
    turned = jnp.concatenate(
        [
            -block[..., pair_count : 2 * pair_count],
            block[..., 0:pair_count],
            -block[..., 3 * pair_count :],
            block[..., 2 * pair_count : 3 * pair_count],
        ],
        axis=-1,
    )
    return block * cosine + turned * sine_table


def channel_norm(rows_in, gain):
    widened = rows_in.astype(jnp.float32)
    return (
        widened * lax.rsqrt(jnp.mean(widened * widened, axis=-1, keepdims=True) + EPS) * gain
    ).astype(jnp.bfloat16)


def body(
    queries,
    keys,
    values,
    documents,
    query_gain,
    key_gain,
    out_weight,
    residual,
    norm_gain,
    up_weight,
    down_weight,
):
    tok_dev = queries.shape[0]
    heads_here = queries.shape[1]
    head_width = queries.shape[2]
    query_group_count = QUERY_HEADS // keys.shape[1]
    kv_index = lax.axis_index("tp") * heads_here // query_group_count
    positions = lax.axis_index("sp") * tok_dev + jnp.arange(tok_dev, dtype=jnp.int32)
    own_keys = lax.dynamic_index_in_dim(keys, kv_index, 1, keepdims=True)
    own_values = lax.dynamic_index_in_dim(values, kv_index, 1, keepdims=False)
    key_rot = rotate(head_norm(own_keys.astype(jnp.float32), key_gain), positions)[:, 0, :].astype(
        jnp.bfloat16
    )
    rotated_query = rotate(head_norm(queries.astype(jnp.float32), query_gain), positions).astype(
        jnp.bfloat16
    )
    scale = head_width ** (-0.5)
    first_doc = documents[0]
    last_doc = documents[tok_dev - 1]
    start_state = (
        jnp.full((tok_dev, heads_here), -1e30, jnp.float32),
        jnp.zeros((tok_dev, heads_here), jnp.float32),
        jnp.zeros((tok_dev, heads_here, head_width), jnp.float32),
    )
    piece_keys = lax.all_gather(key_rot, "sp", axis=0, tiled=True)
    piece_values = lax.all_gather(own_values, "sp", axis=0, tiled=True)
    piece_docs = lax.all_gather(documents, "sp", axis=0, tiled=True)

    def update(state):
        peak, denom, summed = state
        scores = (
            jnp.einsum("qhd,kd->qhk", rotated_query, piece_keys, preferred_element_type=jnp.float32)
            * scale
        )
        allowed = (documents[:, None] == piece_docs[None, :])[:, None, :]
        scores = jnp.where(allowed, scores, -1e30)
        new_peak = jnp.maximum(peak, jnp.max(scores, axis=-1))
        probs = jnp.where(allowed, jnp.exp(scores - new_peak[..., None]), 0.0)
        denom = jnp.sum(probs, axis=-1)
        summed = jnp.einsum(
            "qhk,kd->qhd",
            probs.astype(jnp.bfloat16),
            piece_values,
            preferred_element_type=jnp.float32,
        )
        return (new_peak, denom, summed)

    touches = jnp.logical_and(
        piece_docs[0] <= last_doc, piece_docs[piece_docs.shape[0] - 1] >= first_doc
    )
    peak, denom, summed = lax.cond(touches, update, lambda state: state, start_state)
    attn = (
        (summed / denom[..., None]).reshape(tok_dev, heads_here * head_width).astype(jnp.bfloat16)
    )
    share = tok_dev // lax.axis_size("tp")
    branch = lax.psum(
        jnp.dot(attn, out_weight, preferred_element_type=jnp.float32).astype(jnp.bfloat16), "tp"
    ).astype(jnp.float32)
    whole_rows = (residual.astype(jnp.float32) + branch).astype(jnp.bfloat16)
    normed = channel_norm(whole_rows, norm_gain)
    mid = lax.dynamic_slice_in_dim(whole_rows, lax.axis_index("tp") * share, share, 0)
    raised = jnp.dot(
        normed,
        lax.all_gather(up_weight, "sp", axis=0, tiled=True),
        preferred_element_type=jnp.float32,
    )
    hidden = jnp.square(jax.nn.relu(raised)).astype(jnp.bfloat16)
    terms = lax.dot_general(
        hidden,
        lax.all_gather(down_weight, "sp", axis=0, tiled=True),
        (((1,), (1,)), ((), ())),
        preferred_element_type=jnp.float32,
    )
    mixer = lax.psum_scatter(
        terms.astype(jnp.bfloat16), "tp", scatter_dimension=0, tiled=True
    ).astype(jnp.float32)
    return (mid.astype(jnp.float32) + mixer).astype(jnp.bfloat16)


def solution(mesh):
    in_specs = (
        P("sp", "tp", None),
        P("sp", None, None),
        P("sp", None, None),
        P("sp"),
        P(),
        P(),
        P("tp", None),
        P("sp", None),
        P(),
        P("sp", "tp"),
        P("sp", "tp"),
    )
    out_specs = P(("sp", "tp"), None)
    return jax.shard_map(body, mesh=mesh, in_specs=in_specs, out_specs=out_specs, check_vma=False)
```

profile of v0, /device:TPU:0, one launch (start us, length us, event | category | flops | bytes accessed | tf_op | source)
XLA Modules:
  0.0 500.5 jit_solution(8802338885907431787)
XLA Ops:
  6.5 0.0 copy-start
  6.5 0.0 all-gather.12.cloned.1.call-start
  6.6 1.2 constant_dynamic-slice_fusion.1
  7.8 0.1 fusion.26
  7.9 0.8 fusion.27
  8.6 0.2 slice_negate_fusion.3
  8.8 0.1 fusion.30
  9.0 1.9 fusion.29
  10.9 0.0 all-gather.12.cloned.1.call-update
  10.9 0.0 all-gather.14.cloned.1.call-start
  11.0 1.0 constant_dynamic-slice_fusion
  12.0 0.6 copy.28
  12.7 0.0 all-gather.14.cloned.1.call-update
  12.7 0.0 all-reduce.2.cloned.1.call-start
  12.7 42.7 %all-gather.2 = s32[16,1,256]{2,1,0:T(1,128)S(1)} all-gather(s32[1,1,256]{2,1,0:T(1,128)} %bitcast.27), channel_id=1, replica_groups=mesh['sp'=16,'tp'=2] {'sp'}, dimensions={0}, use_global_device_ids=true | all-gather | bytes 17408 | tf_op jit(solution)/shard_map/all_gather | solution.py:83
  55.5 1.3 fusion.39
  56.8 0.7 fusion.38
  60.0 0.6 fusion.33
  60.6 1.2 fusion.22
  61.8 1.2 fusion.23
  63.0 0.5 slice_negate_fusion.1
  63.4 1.6 fusion.25
  65.0 3.9 all-gather.12.cloned.1.call-done
  68.9 56.7 %all-gather.14.cloned.1.call-done = bf16[4096,1,128]{2,0,1:T(8,128)(2,1)} async-done(((bf16[256,1,128]{2,0,1:T(8,128)(2,1)}), bf16[4096,1,128]{2,0,1:T(8,128)(2,1)}) %all-gather.14.cloned.1.call-update) | async-done | bytes 1048592 | tf_op jit(solution)/shard_map/all_gather | solution.py:82
  125.6 0.0 copy-done.1
  125.6 15.6 %conditional.1 = (f32[256,4]{0,1:T(4,128)S(1)}, f32[256,4,128]{0,2,1:T(8,128)S(1)}) conditional(s32[]{:T(128)} %bitcast.4, () %tuple.13, (s32[256]{0:T(256)S(1)}, s32[4096]{0:T(1024)S(1)}, bf16[256,4,128]{2,0,1:T(8,128)(2,1)S(1)}, bf16[4096,128]{1,0:T(8,128)(2,1)}, bf16[4096,128]{1,0:T(8,128)(2,1)}) %tuple.50), branch_computations={%region_2.3_spmd, %region_3.6_spmd} | conditional | flops 2203057152 | bytes 61645868 | solution.py:107
  125.6 0.6 broadcast_compare_fusion
  126.3 0.0 copy-start.2
  126.3 4.8 fusion
  131.0 0.0 copy-done.2
  131.1 4.9 fusion.3
  136.0 5.1 %fusion.2 = f32[256,4]{0,1:T(4,128)S(1)} fusion(f32[256,4,4096]{2,0,1:T(8,128)S(1)} %get-tuple-element.28, f32[256,4]{0,1:T(4,128)S(1)} %broadcast_maximum_fusion, pred[256,4096]{1,0:T(8,128)(4,1)S(1)} %broadcast_compare_fusion), kind=kLoop, calls=%fused_computation.4 | loop fusion | flops 20970496 | bytes 17833984 | tf_op jit(solution)/shard_map/cond/branch_1_fun/reduce_sum | solution.py:95
  141.3 0.0 copy-done
  141.3 1.7 convolution_convert_fusion
  143.0 0.0 all-reduce.2.cloned.1.call-update
  143.0 0.0 all-gather.10.cloned.1.call-start
  143.1 0.5 all-gather.10.cloned.1.call-update
  143.6 0.0 all-gather.8.cloned.1.call-start
  143.6 0.5 all-gather.8.cloned.1.call-update
  144.2 0.0 reduce-scatter.2.cloned.1.call-start
  144.2 17.2 %all-reduce.2.cloned.1.call-done = bf16[256,2048]{1,0:T(8,128)(2,1)} async-done(((bf16[256,2048]{1,0:T(8,128)(2,1)}), bf16[256,2048]{1,0:T(8,128)(2,1)}) %all-reduce.2.cloned.1.call-update) | async-done | bytes 1048592 | tf_op jit(solution)/shard_map/psum | solution.py:112
  161.4 2.0 fusion.14
  163.5 153.2 %all-gather.10.cloned.1.call-done = bf16[2048,3072]{1,0:T(8,128)(2,1)} async-done(((bf16[128,3072]{1,0:T(8,128)(2,1)}), bf16[2048,3072]{1,0:T(8,128)(2,1)}) %all-gather.10.cloned.1.call-update) | async-done | bytes 12582928 | tf_op jit(solution)/shard_map/all_gather | solution.py:126
  316.7 152.3 %all-gather.8.cloned.1.call-done = bf16[2048,3072]{1,0:T(8,128)(2,1)} async-done(((bf16[128,3072]{1,0:T(8,128)(2,1)}), bf16[2048,3072]{1,0:T(8,128)(2,1)}) %all-gather.8.cloned.1.call-update) | async-done | bytes 12582928 | tf_op jit(solution)/shard_map/all_gather | solution.py:120
  468.9 16.0 %convolution_convert_fusion.1 = bf16[256,2048]{1,0:T(8,128)(2,1)} fusion(bf16[2048,3072]{1,0:T(8,128)(2,1)} %all-gather.10.cloned.1.call-done, bf16[2048,3072]{1,0:T(8,128)(2,1)} %all-gather.8.cloned.1.call-done, bf16[256,2048]{1,0:T(8,128)(2,1)S(1)} %get-tuple-element.26, f32[2048]{0:T(1024)S(1)} %copy-done.3, f32[256]{0:T(256)S(1)} %add_rsqrt_fusion.1), kind=kOutput, calls=%fused_computation.21 | convolution fusion | flops 6447431680 | bytes 27272192 | tf_op jit(solution)/shard_map/dot_general | solution.py:124
  485.0 0.0 reduce-scatter.2.cloned.1.call-update
  485.0 6.7 %reduce-scatter.2.cloned.1.call-done = bf16[128,2048]{1,0:T(8,128)(2,1)} async-done(((bf16[256,2048]{1,0:T(8,128)(2,1)}), bf16[128,2048]{1,0:T(8,128)(2,1)}) %reduce-scatter.2.cloned.1.call-update) | async-done | bytes 524304 | tf_op jit(solution)/shard_map/reduce_scatter | solution.py:130
  491.7 2.0 add_convert_fusion.1
  (10 shorter events, 0.1 us)
Async XLA Ops:
  6.5 134.7 %copy-start = (bf16[512,2048]{1,0:T(8,128)(2,1)S(1)}, bf16[512,2048]{1,0:T(8,128)(2,1)}, u32[]{:S(2)}) copy-start(bf16[512,2048]{1,0:T(8,128)(2,1)} %param.19) | copy-start | bytes 6291460
  6.5 119.1 %copy-start.1 = (s32[256]{0:T(256)S(1)}, s32[256]{0:T(256)}, u32[]{:S(2)}) copy-start(s32[256]{0:T(256)} %param.16) | copy-start | bytes 3076
  6.5 62.3 %all-gather.12.cloned.1.call-start = ((), (), s32[]{:S(2)}) async-start(), calls=%async_computation.5 | async-start | bytes 1114112 | tf_op jit(solution)/shard_map/all_gather | solution.py:81
  10.9 114.7 %all-gather.14.cloned.1.call-start = ((), (), s32[]{:S(2)}) async-start(), calls=%async_computation.6 | async-start | bytes 1114112 | tf_op jit(solution)/shard_map/all_gather | solution.py:82
  12.7 148.7 %all-reduce.2.cloned.1.call-start = ((), (), s32[]{:S(2)}) async-start(), calls=%async_computation.1 | async-start | bytes 2097152 | tf_op jit(solution)/shard_map/psum | solution.py:112
  125.6 343.3 %copy-start.3 = (f32[2048]{0:T(1024)S(1)}, f32[2048]{0:T(1024)}, u32[]{:S(2)}) copy-start(f32[2048]{0:T(1024)} %param.21) | copy-start | bytes 24580
  126.3 4.8 copy-start.2
  143.0 173.7 %all-gather.10.cloned.1.call-start = ((), (), s32[]{:S(2)}) async-start(), calls=%async_computation.3 | async-start | bytes 13369344 | tf_op jit(solution)/shard_map/all_gather | solution.py:126
  143.6 325.3 %all-gather.8.cloned.1.call-start = ((), (), s32[]{:S(2)}) async-start(), calls=%async_computation.2 | async-start | bytes 13369344 | tf_op jit(solution)/shard_map/all_gather | solution.py:120
  144.2 347.5 %reduce-scatter.2.cloned.1.call-start = ((), (), s32[]{:S(2)}) async-start(), calls=%async_computation.4 | async-start | bytes 1572864 | tf_op jit(solution)/shard_map/reduce_scatter | solution.py:130
Sparse Core Ops, SparseCore 0:
  11.0 57.7 all-gather.11
  71.6 53.9 all-gather.13
  143.1 18.2 all-reduce.1
  164.0 152.5 all-gather.9
  319.3 149.5 all-gather.7
  485.1 6.5 reduce-scatter.1
where the time goes:
time: 501 us
  waiting for transfers between devices  391 us (78%)
  blocking collectives  42.7 us (9%)
  matrix products  27.4 us (5%)
  other arithmetic  17.9 us (4%)
  between operations  16.1 us (3%)
    all_gather x1, waiting for transfers between devices, body(): lax.all_gather(down_weight, 'sp', axis=0, tiled=True)  153 us
    all_gather x1, waiting for transfers between devices, body(): lax.all_gather(up_weight, 'sp', axis=0, tiled=True)  152 us
    all_gather x1, waiting for transfers between devices, body(): piece_values = lax.all_gather(own_values, 'sp', axis=0, tiled=True)  56.7 us
    all_gather x1, blocking collectives, body(): piece_docs = lax.all_gather(documents, 'sp', axis=0, tiled=True)  42.7 us
    psum x1, waiting for transfers between devices, body(): lax.psum(jnp.dot(attn, out_weight, preferred_element_type=jnp.float32).as...  17.2 us
    dot_general x1, matrix products, body(): lax.dot_general(hidden, lax.all_gather(down_weight, 'sp', axis=0, tiled=T...  16 us
  transfers between devices with their start and end apart: 6, of which 6 were waited for; matrix products, arithmetic and copies ran while one was open for 2% of the time, Pallas kernels for 0%

commit v1 on v0

--- a/solution.py
+++ b/solution.py
@@ -1,6 +1,10 @@
+import functools
+
 import jax
 import jax.numpy as jnp
 from jax import lax
+from jax.experimental import pallas as pl
+from jax.experimental.pallas import tpu as pltpu
 from jax.sharding import PartitionSpec as P
 
 QUERY_HEADS = 8
@@ -133,6 +137,317 @@
     return (mid.astype(jnp.float32) + mixer).astype(jnp.bfloat16)
 
 
+MESH = pl.DeviceIdType.MESH
+NT = (((1,), (1,)), ((), ()))
+F32 = jnp.float32
+BF16 = jnp.bfloat16
+
+
+def layer_kernel(
+    q_ref, kv_ref, drow_ref, dcol_ref, ow_ref, res_ref, gain_ref, up_ref, down_ref, out_ref,
+    kv_all, doc_all, attn, wup, wdown, part, part_in, mid, norm_all, hidden, outs, outs_in, sums,
+    final_in, kv_s, kv_r, dc_s, dc_r, w_s, w_r, loc_s, p_s, p_r, n_s, n_r, o_s, o_r, f_s, f_r,
+):
+    heads, rows, width = q_ref.shape
+    half = rows // 2
+    depth, cols = wup.shape[1], wup.shape[2]
+    model = ow_ref.shape[1]
+    sp, core = lax.axis_index("sp"), lax.axis_index("tp")
+    n_z = lax.axis_size("sp") // 4
+    x, y, z = sp % 2, (sp // 2) % 2, sp // 4
+
+    def at(dx, dy, r):
+        return ((z + r) % n_z * 2 + (y + dy) % 2) * 2 + (x + dx) % 2
+
+    def mate(rc):
+        return (((z // 2) * 2 + (z + rc // 2) % 2) * 2 + y) * 2 + (x + rc) % 2
+
+    def rank(spi):
+        return (spi // 4) % 2 * 2 + spi % 2
+
+    sent = []
+
+    def send(src, dst, ss, rs, spi, tpi):
+        c = pltpu.make_async_remote_copy(
+            src_ref=src, dst_ref=dst, send_sem=ss, recv_sem=rs,
+            device_id=(spi, tpi), device_id_type=MESH,
+        )
+        c.start()
+        sent.append(c)
+
+    def arrive(dst, ss, rs):
+        pltpu.make_async_remote_copy(
+            src_ref=dst, dst_ref=dst, send_sem=ss, recv_sem=rs,
+            device_id=(sp, 1 - core), device_id_type=MESH,
+        ).wait_recv()
+
+    barrier = pltpu.get_barrier_semaphore()
+    peers = [(at(dx, 0, k), core) for dx in (0, 1) for k in range(n_z) if dx or k]
+    peers += [(at(0, 1, 0), core), (sp, 1 - core)]
+    for p in peers:
+        pl.semaphore_signal(barrier, inc=1, device_id=p, device_id_type=MESH)
+    pl.semaphore_wait(barrier, len(peers))
+
+    def slot(dx, dy, r):
+        return (dx * 2 + dy) * n_z + r
+
+    def send_kv(src_slot, dst_slot, spi):
+        src = kv_ref if src_slot is None else kv_all.at[src_slot]
+        dsrc = drow_ref if src_slot is None else doc_all.at[src_slot]
+        i = dst_slot
+        send(src, kv_all.at[dst_slot], kv_s.at[i], kv_r.at[i], spi, core)
+        send(dsrc, doc_all.at[dst_slot], dc_s.at[i], dc_r.at[i], spi, core)
+
+    def wait_kv(i):
+        arrive(kv_all.at[i], kv_s.at[i], kv_r.at[i])
+        arrive(doc_all.at[i], dc_s.at[i], dc_r.at[i])
+
+    weights = ((up_ref, wup), (down_ref, wdown))
+
+    def send_weight(w, dx, k):
+        src, dst = weights[w]
+        target = at(dx, 0, k)
+        block = src.at[:, pl.ds(pl.multiple_of(rank(target) * cols, 128), cols)]
+        i = dx * n_z + (n_z - k) % n_z
+        if dx or k:
+            send(block, dst.at[sp], w_s.at[w, i], w_r.at[w, i], target, core)
+
+    def forward_weight(w, i):
+        dst = weights[w][1]
+        owner = at(i // n_z, 0, i % n_z)
+        if i:
+            arrive(dst.at[owner], w_s.at[w, i], w_r.at[w, i])
+        j = 2 * n_z + i
+        send(dst.at[owner], dst.at[owner], w_s.at[w, j], w_r.at[w, j], at(0, 1, 0), core)
+
+    def last_weight(w):
+        dst = weights[w][1]
+        for i in range(2 * n_z):
+            owner = at(i // n_z, 1, i % n_z)
+            arrive(dst.at[owner], w_s.at[w, 2 * n_z + i], w_r.at[w, 2 * n_z + i])
+
+    for k in range(1, n_z):
+        send_kv(None, slot(0, 0, n_z - k), at(0, 0, k))
+    send_kv(None, slot(1, 0, 0), at(1, 0, 0))
+    send_kv(None, slot(0, 1, 0), at(0, 1, 0))
+    own = []
+    for w in (0, 1):
+        src, dst = weights[w]
+        block = src.at[:, pl.ds(pl.multiple_of(rank(sp) * cols, 128), cols)]
+        own.append(pltpu.make_async_copy(block, dst.at[sp], loc_s.at[w]))
+    own.append(pltpu.make_async_copy(kv_ref, kv_all.at[0], loc_s.at[2]))
+    own.append(pltpu.make_async_copy(drow_ref, doc_all.at[0], loc_s.at[3]))
+    for c in own:
+        c.start()
+    near = sorted(range(1, n_z), key=lambda r: min(r, n_z - r))
+    for k in near:
+        send_weight(0, 0, k)
+    for r in near:
+        wait_kv(slot(0, 0, r))
+        send_kv(slot(0, 0, r), slot(1, 0, r), at(1, 0, 0))
+        send_kv(slot(0, 0, r), slot(0, 1, r), at(0, 1, 0))
+    for r in [0] + near:
+        wait_kv(slot(1, 0, r))
+        if r < n_z // 2:
+            send_kv(slot(1, 0, r), slot(1, 1, r), at(0, 1, 0))
+        wait_kv(slot(0, 1, r))
+        if r >= n_z // 2:
+            send_kv(slot(0, 1, r), slot(1, 1, r), at(1, 0, 0))
+    for c in own:
+        c.wait()
+    for k in [0] + near:
+        send_weight(0, 1, k)
+    for k in near:
+        send_weight(1, 0, k)
+    for k in [0] + near:
+        send_weight(1, 1, k)
+    order = [dx * n_z + r for dx in (0, 1) for r in [0] + near]
+    forward_weight(0, order[0])
+    for r in range(n_z):
+        wait_kv(slot(1, 1, r))
+
+    scale = width ** (-0.5)
+    n_slots = kv_all.shape[0]
+    todo = order[1:]
+    for h in range(heads):
+
+        def step(i, state):
+            peak, denom, acc = state
+            scores = lax.dot_general(q_ref[h], kv_all[i, 0], NT, preferred_element_type=F32) * scale
+            allowed = dcol_ref[...] == doc_all[i]
+            scores = jnp.where(allowed, scores, -1e30)
+            new_peak = jnp.maximum(peak, jnp.max(scores, axis=-1, keepdims=True))
+            probs = jnp.where(allowed, jnp.exp(scores - new_peak), 0.0)
+            decay = jnp.exp(peak - new_peak)
+            denom = denom * decay + jnp.sum(probs, axis=-1, keepdims=True)
+            acc = acc * decay + jnp.dot(
+                probs.astype(BF16), kv_all[i, 1], preferred_element_type=F32
+            )
+            return new_peak, denom, acc
+
+        state = (
+            jnp.full((rows, 1), -1e30, F32),
+            jnp.zeros((rows, 1), F32),
+            jnp.zeros((rows, width), F32),
+        )
+        peak, denom, acc = lax.fori_loop(0, n_slots, step, state)
+        attn[:, h * width : (h + 1) * width] = (acc / denom).astype(BF16)
+        if h >= heads // 2:
+            for i in todo[:2]:
+                forward_weight(0, i)
+            todo = todo[2:]
+
+    tile = 256
+
+    @pl.loop(0, model // tile)
+    def _(t):
+        lanes = pl.ds(pl.multiple_of(t * tile, tile), tile)
+        p = jnp.dot(attn[...], ow_ref[:, lanes], preferred_element_type=F32).astype(BF16)
+        part[0, :, lanes] = p[:half]
+        part[1, :, lanes] = p[half:]
+
+    send(part.at[1 - core], part_in, p_s, p_r, sp, 1 - core)
+    arrive(part_in, p_s, p_r)
+    start = pl.ds(pl.multiple_of(core * half, half), half)
+    group = 32
+
+    @pl.loop(0, half // group)
+    def _(t):
+        rws = pl.ds(pl.multiple_of(t * group, group), group)
+        branch = part[core, rws].astype(F32) + part_in[rws].astype(F32)
+        rres = pl.ds(pl.multiple_of(core * half + t * group, group), group)
+        m = (res_ref[rres].astype(F32) + branch).astype(BF16)
+        mid[rws] = m
+        wide = m.astype(F32)
+        inv = lax.rsqrt(jnp.mean(wide * wide, axis=-1, keepdims=True) + EPS)
+        norm_all[0, 0, rws] = (wide * inv * gain_ref[...]).astype(BF16)
+
+    for rc in (3, 1, 2):
+        send(norm_all.at[0, 0], norm_all.at[rc, 0], n_s.at[rc], n_r.at[rc], mate(rc), core)
+    send(norm_all.at[0, 0], norm_all.at[0, 1], n_s.at[4], n_r.at[4], sp, 1 - core)
+    for i in todo:
+        forward_weight(0, i)
+    for i in order[:1] + order[1:5]:
+        forward_weight(1, i)
+    for rc in (1, 2, 3):
+        arrive(norm_all.at[rc, 0], n_s.at[rc], n_r.at[rc])
+        j = 4 + rc
+        send(norm_all.at[rc, 0], norm_all.at[rc, 1], n_s.at[j], n_r.at[j], sp, 1 - core)
+    for i in order[5:]:
+        forward_weight(1, i)
+    last_weight(0)
+    for rc in range(4):
+        arrive(norm_all.at[rc, 1], n_s.at[4 + rc], n_r.at[4 + rc])
+
+    @pl.loop(0, 4 * (cols // tile))
+    def _(t):
+        rc, c = t // (cols // tile), t % (cols // tile)
+        lanes = pl.ds(pl.multiple_of(c * tile, tile), tile)
+        tokens = norm_all[rc].reshape(rows, model)
+        w = wup[:, :, lanes].reshape(model, tile)
+        raised = jnp.dot(tokens, w, preferred_element_type=F32)
+        hidden[rc, :, lanes] = jnp.square(jnp.maximum(raised, 0.0)).astype(BF16)
+
+    last_weight(1)
+    blocks = tile // depth
+
+    for rc in (3, 1, 2, 0):
+
+        @pl.loop(0, model // tile)
+        def _(t):
+            lanes = pl.ds(pl.multiple_of(t * tile, tile), tile)
+            w = wdown[pl.ds(t * blocks, blocks)].reshape(tile, cols)
+            o = lax.dot_general(hidden[rc], w, NT, preferred_element_type=F32).astype(BF16)
+            outs[rc, 0, :, lanes] = o[:half]
+            outs[rc, 1, :, lanes] = o[half:]
+
+        send(outs.at[rc, 1], outs_in.at[rc], o_s.at[rc], o_r.at[rc], sp, 1 - core)
+
+    for rc in (3, 1, 2, 0):
+        arrive(outs_in.at[rc], o_s.at[rc], o_r.at[rc])
+        if rc:
+
+            @pl.loop(0, half // group)
+            def _(t):
+                rws = pl.ds(pl.multiple_of(t * group, group), group)
+                sums[rc - 1, rws] = (
+                    outs[rc, 0, rws].astype(F32) + outs_in[rc, rws].astype(F32)
+                ).astype(BF16)
+
+            send(sums.at[rc - 1], final_in.at[rc - 1], f_s.at[rc], f_r.at[rc], mate(rc), core)
+    for rc in (1, 2, 3):
+        arrive(final_in.at[rc - 1], f_s.at[rc], f_r.at[rc])
+
+    @pl.loop(0, half // group)
+    def _(t):
+        rws = pl.ds(pl.multiple_of(t * group, group), group)
+        total = outs[0, 0, rws].astype(F32) + outs_in[0, rws].astype(F32)
+        for rc in range(3):
+            total += final_in[rc, rws].astype(F32)
+        out_ref[rws] = (mid[rws].astype(F32) + total).astype(BF16)
+
+    for c in sent:
+        c.wait_send()
+
+
+def fused_body(
+    queries, keys, values, documents, query_gain, key_gain, out_weight, residual, norm_gain,
+    up_weight, down_weight,
+):
+    rows, heads, width = queries.shape
+    n_sp = lax.axis_size("sp")
+    model = residual.shape[1]
+    depth, cols = up_weight.shape[0], up_weight.shape[1] // 4
+    half = rows // 2
+    kv_index = lax.axis_index("tp") * heads // (QUERY_HEADS // keys.shape[1])
+    positions = lax.axis_index("sp") * rows + jnp.arange(rows, dtype=jnp.int32)
+    own_keys = lax.dynamic_index_in_dim(keys, kv_index, 1, keepdims=True)
+    own_values = lax.dynamic_index_in_dim(values, kv_index, 1, keepdims=False)
+    key_rot = rotate(head_norm(own_keys.astype(F32), key_gain), positions)[:, 0, :].astype(BF16)
+    query_rot = rotate(head_norm(queries.astype(F32), query_gain), positions).astype(BF16)
+    vm = pl.BlockSpec(memory_space=pltpu.VMEM)
+    dma = pltpu.SemaphoreType.DMA
+    token = (half, model)
+    return pl.pallas_call(
+        layer_kernel,
+        out_shape=jax.ShapeDtypeStruct(token, BF16),
+        in_specs=[vm] * 9,
+        out_specs=vm,
+        scratch_shapes=[
+            pltpu.VMEM((n_sp, 2, rows, width), BF16),
+            pltpu.VMEM((n_sp, 1, rows), jnp.int32),
+            pltpu.VMEM((rows, heads * width), BF16),
+            pltpu.VMEM((n_sp, depth, cols), BF16),
+            pltpu.VMEM((n_sp, depth, cols), BF16),
+            pltpu.VMEM((2,) + token, BF16),
+            pltpu.VMEM(token, BF16),
+            pltpu.VMEM(token, BF16),
+            pltpu.VMEM((4, 2) + token, BF16),
+            pltpu.VMEM((4, rows, cols), BF16),
+            pltpu.VMEM((4, 2) + token, BF16),
+            pltpu.VMEM((4,) + token, BF16),
+            pltpu.VMEM((3,) + token, BF16),
+            pltpu.VMEM((3,) + token, BF16),
+            dma((n_sp,)), dma((n_sp,)), dma((n_sp,)), dma((n_sp,)),
+            dma((2, n_sp)), dma((2, n_sp)), dma((4,)),
+            dma, dma, dma((8,)), dma((8,)), dma((4,)), dma((4,)), dma((4,)), dma((4,)),
+        ],
+        compiler_params=pltpu.CompilerParams(
+            collective_id=0, has_side_effects=True, vmem_limit_bytes=60 * 1024 * 1024
+        ),
+    )(
+        query_rot.transpose(1, 0, 2),
+        jnp.stack([key_rot, own_values]),
+        documents[None, :],
+        documents[:, None],
+        out_weight,
+        residual,
+        norm_gain[None, :],
+        up_weight,
+        down_weight,
+    )
+
+
 def solution(mesh):
     in_specs = (
         P("sp", "tp", None),
@@ -148,4 +463,5 @@
         P("sp", "tp"),
     )
     out_specs = P(("sp", "tp"), None)
-    return jax.shard_map(body, mesh=mesh, in_specs=in_specs, out_specs=out_specs, check_vma=False)
+    fused = mesh.shape["tp"] == 2 and mesh.shape["sp"] == 16
+    return jax.shard_map(fused_body if fused else body, mesh=mesh, in_specs=in_specs, out_specs=out_specs, check_vma=False)

time: 501 us -> 181 us (0.36)
  waiting for transfers between devices: 391 us -> 0 us
  Pallas kernels: 0 us -> 171 us
  blocking collectives: 42.7 us -> 0 us
  matrix products: 27.4 us -> 0 us
  between operations: 16.1 us -> 0.14 us
  other arithmetic: 17.9 us -> 5.26 us
    all_gather x4 -> x0, waiting for transfers between devices: 366 us -> none  [the longest x1 153 us: body(): lax.all_gather(down_weight, 'sp', axis=0, tiled=True)]
    pallas_call x0 -> x1, Pallas kernels: none -> 171 us  [fused_body(): pl.pallas_call(layer_kernel, out_shape=jax.ShapeDtypeStruct(token, BF16),...]
    all_gather x1 -> x0, blocking collectives: 42.7 us -> none  [body(): piece_docs = lax.all_gather(documents, 'sp', axis=0, tiled=True)]
    dot_general x3 -> x0, matrix products: 22.5 us -> none  [the longest x1 16 us: body(): lax.dot_general(hidden, lax.all_gather(down_weight, 'sp', axis=0, tiled=T...]
    psum x1 -> x0, waiting for transfers between devices: 17.2 us -> none  [body(): lax.psum(jnp.dot(attn, out_weight, preferred_element_type=jnp.float32).as...]
    reduce_sum x2 -> x0, other arithmetic: 7.11 us -> none  [the longest x1 5.07 us: update(): denom = jnp.sum(probs, axis=-1)]
    reduce_scatter x1 -> x0, waiting for transfers between devices: 6.73 us -> none  [body(): lax.psum_scatter(terms.astype(jnp.bfloat16), 'tp', scatter_dimension=0, t...]
  transfers between devices with their start and end apart: 6 -> 0, of which waited for: 6 -> 0; matrix products, arithmetic and copies ran while one was open for 2% -> 0% of each run, Pallas kernels for 0% -> 0%
where the time goes in v1:
time: 181 us; the launch traced here: 180 us
  Pallas kernels  171 us (94%)
  other arithmetic  5.26 us (3%)
  local copies, waits for them, and re-layouts  3.97 us (2%)
    pallas_call x1, Pallas kernels, fused_body(): pl.pallas_call(layer_kernel, out_shape=jax.ShapeDtypeStruct(token, BF16),...  171 us

profile of v1, /device:TPU:0, one launch (start us, length us, event | category | flops | bytes accessed | tf_op | source)
XLA Modules:
  0.0 180.5 jit_solution(4227937807016906134)
XLA Ops:
  0.0 0.0 copy-start.2
  0.0 1.3 constant_dynamic-slice_fusion
  1.3 0.0 copy-start
  1.3 0.0 copy-start.3
  1.3 0.1 fusion.5
  1.4 0.8 fusion.6
  2.2 0.2 slice_negate_fusion.3
  2.4 0.1 fusion.10
  2.5 0.0 copy-done.2
  2.5 0.6 fusion.9
  3.2 0.7 pad_maximum_fusion.2.kv_ref
  3.9 0.6 fusion.13
  4.4 0.0 copy-done
  4.4 0.2 fusion
  4.7 0.0 copy-done.3
  4.7 0.2 fusion.1
  4.9 0.5 slice_negate_fusion.1
  5.4 0.0 copy-start.1
  5.4 1.3 fusion.4.q_ref
  6.7 0.0 copy-done.1
  6.7 0.8 copy.17.dcol_ref
  7.5 171.1 %shard_map.109 = bf16[128,2048]{1,0:T(8,128)(2,1)} custom-call(bf16[4,256,128]{2,1,0:T(8,128)(2,1)} %fusion.4.q_ref, bf16[2,256,128]{2,1,0:T(8,128)(2,1)} %pad_maximum_fusion.2.kv_ref, s32[1,256]{1,0:T(1,128)} %bitcast.16, s32[256,1]{1,0:T(8,128)} %copy.17.dcol_ref, bf16[512,2048]{1,0:T(8,128)(2,1)} %ow_ref.1, bf16[256,2048]{1,0:T(8,128)(2,1)} %res_ref.1, ...), custom_call_target="tpu_custom_call" | custom-call | tf_op jit(solution)/shard_map/pallas_call | solution.py:411
  178.6 1.9 %copy.31 = bf16[128,2048]{1,0:T(8,128)(2,1)} copy(bf16[128,2048]{1,0:T(8,128)(2,1)} %shard_map.109) | data formatting | bytes 1048576
  (5 shorter events, 0.0 us)
Async XLA Ops:
  0.0 2.5 %copy-start.2 = (f32[128]{0:T(128)S(1)}, f32[128]{0:T(128)}, u32[]{:S(2)}) copy-start(f32[128]{0:T(128)} %param.16) | copy-start | bytes 1540
  1.3 3.2 %copy-start = (bf16[256,4,128]{2,1,0:T(4,128)(2,1)S(1)}, bf16[256,4,128]{2,1,0:T(4,128)(2,1)}, u32[]{:S(2)}) copy-start(bf16[256,4,128]{2,1,0:T(4,128)(2,1)} %param.11) | copy-start | bytes 786436
  1.3 3.4 %copy-start.3 = (f32[128]{0:T(128)S(1)}, f32[128]{0:T(128)}, u32[]{:S(2)}) copy-start(f32[128]{0:T(128)} %param.15) | copy-start | bytes 1540
  5.4 1.3 copy-start.1

commit v2 on v1

--- a/solution.py
+++ b/solution.py
@@ -141,14 +141,17 @@
 NT = (((1,), (1,)), ((), ()))
 F32 = jnp.float32
 BF16 = jnp.bfloat16
+LOG2E = 1.4426950408889634
+APART = 1024.0
 
 
 def layer_kernel(
-    q_ref, kv_ref, drow_ref, dcol_ref, ow_ref, res_ref, gain_ref, up_ref, down_ref, out_ref,
-    kv_all, doc_all, attn, wup, wdown, part, part_in, mid, norm_all, hidden, outs, outs_in, sums,
+    q_ref, key_ref, val_ref, ow_ref, res_ref, gain_ref, up_ref, down_ref, out_ref,
+    key_all, val_all, attn, wup, wdown, part, part_in, mid, norm_all, hidden, outs, outs_in, sums,
     final_in, kv_s, kv_r, dc_s, dc_r, w_s, w_r, loc_s, p_s, p_r, n_s, n_r, o_s, o_r, f_s, f_r,
 ):
-    heads, rows, width = q_ref.shape
+    heads, rows = q_ref.shape[:2]
+    used, width = key_ref.shape[0], val_ref.shape[1]
     half = rows // 2
     depth, cols = wup.shape[1], wup.shape[2]
     model = ow_ref.shape[1]
@@ -191,16 +194,21 @@
     def slot(dx, dy, r):
         return (dx * 2 + dy) * n_z + r
 
-    def send_kv(src_slot, dst_slot, spi):
-        src = kv_ref if src_slot is None else kv_all.at[src_slot]
-        dsrc = drow_ref if src_slot is None else doc_all.at[src_slot]
-        i = dst_slot
-        send(src, kv_all.at[dst_slot], kv_s.at[i], kv_r.at[i], spi, core)
-        send(dsrc, doc_all.at[dst_slot], dc_s.at[i], dc_r.at[i], spi, core)
+    def key_at(i):
+        return key_all.at[i, pl.ds(0, used)]
+
+    def val_at(i):
+        return val_all.at[i, :, pl.ds(0, width)]
+
+    def send_kv(src_slot, i, spi):
+        ksrc = key_ref if src_slot is None else key_at(src_slot)
+        vsrc = val_ref if src_slot is None else val_at(src_slot)
+        send(ksrc, key_at(i), kv_s.at[i], kv_r.at[i], spi, core)
+        send(vsrc, val_at(i), dc_s.at[i], dc_r.at[i], spi, core)
 
     def wait_kv(i):
-        arrive(kv_all.at[i], kv_s.at[i], kv_r.at[i])
-        arrive(doc_all.at[i], dc_s.at[i], dc_r.at[i])
+        arrive(key_at(i), kv_s.at[i], kv_r.at[i])
+        arrive(val_at(i), dc_s.at[i], dc_r.at[i])
 
     weights = ((up_ref, wup), (down_ref, wdown))
 
@@ -235,13 +243,21 @@
         src, dst = weights[w]
         block = src.at[:, pl.ds(pl.multiple_of(rank(sp) * cols, 128), cols)]
         own.append(pltpu.make_async_copy(block, dst.at[sp], loc_s.at[w]))
-    own.append(pltpu.make_async_copy(kv_ref, kv_all.at[0], loc_s.at[2]))
-    own.append(pltpu.make_async_copy(drow_ref, doc_all.at[0], loc_s.at[3]))
+    own.append(pltpu.make_async_copy(key_ref, key_at(0), loc_s.at[2]))
+    own.append(pltpu.make_async_copy(val_ref, val_at(0), loc_s.at[3]))
     for c in own:
         c.start()
+    order = [dx * n_z + r for dx in (0, 1) for r in (0, 1, n_z - 1, *range(2, n_z - 1))]
     near = sorted(range(1, n_z), key=lambda r: min(r, n_z - r))
     for k in near:
         send_weight(0, 0, k)
+    n_slots = key_all.shape[0]
+
+    @pl.loop(0, n_slots)
+    def _(i):
+        key_all[i, used:, :] = jnp.zeros((key_all.shape[1] - used, rows), BF16)
+        val_all[i, :, width:] = jnp.ones((rows, val_all.shape[2] - width), BF16)
+
     for r in near:
         wait_kv(slot(0, 0, r))
         send_kv(slot(0, 0, r), slot(1, 0, r), at(1, 0, 0))
@@ -259,43 +275,35 @@
         send_weight(0, 1, k)
     for k in near:
         send_weight(1, 0, k)
-    for k in [0] + near:
-        send_weight(1, 1, k)
-    order = [dx * n_z + r for dx in (0, 1) for r in [0] + near]
-    forward_weight(0, order[0])
+    for i in order[:3]:
+        forward_weight(0, i)
     for r in range(n_z):
         wait_kv(slot(1, 1, r))
 
-    scale = width ** (-0.5)
-    n_slots = kv_all.shape[0]
-    todo = order[1:]
+    todo = order[3:]
+    span = 4
     for h in range(heads):
 
-        def step(i, state):
-            peak, denom, acc = state
-            scores = lax.dot_general(q_ref[h], kv_all[i, 0], NT, preferred_element_type=F32) * scale
-            allowed = dcol_ref[...] == doc_all[i]
-            scores = jnp.where(allowed, scores, -1e30)
-            new_peak = jnp.maximum(peak, jnp.max(scores, axis=-1, keepdims=True))
-            probs = jnp.where(allowed, jnp.exp(scores - new_peak), 0.0)
-            decay = jnp.exp(peak - new_peak)
-            denom = denom * decay + jnp.sum(probs, axis=-1, keepdims=True)
-            acc = acc * decay + jnp.dot(
-                probs.astype(BF16), kv_all[i, 1], preferred_element_type=F32
-            )
-            return new_peak, denom, acc
-
-        state = (
-            jnp.full((rows, 1), -1e30, F32),
-            jnp.zeros((rows, 1), F32),
-            jnp.zeros((rows, width), F32),
-        )
-        peak, denom, acc = lax.fori_loop(0, n_slots, step, state)
-        attn[:, h * width : (h + 1) * width] = (acc / denom).astype(BF16)
-        if h >= heads // 2:
-            for i in todo[:2]:
-                forward_weight(0, i)
-            todo = todo[2:]
+        def step(g, state):
+            peak, acc = state
+            scores = [
+                jnp.dot(q_ref[h], key_all[g * span + j], preferred_element_type=F32)
+                for j in range(span)
+            ]
+            highest = functools.reduce(jnp.maximum, scores)
+            new_peak = jnp.maximum(peak, jnp.max(highest, axis=-1, keepdims=True))
+            acc = acc * jnp.exp2(peak - new_peak)
+            for j in range(span):
+                probs = jnp.exp2(scores[j] - new_peak).astype(BF16)
+                acc += jnp.dot(probs, val_all[g * span + j], preferred_element_type=F32)
+            return new_peak, acc
+
+        state = (jnp.full((rows, 1), -1e30, F32), jnp.zeros((rows, 2 * width), F32))
+        _, acc = lax.fori_loop(0, n_slots // span, step, state)
+        attn[:, h * width : (h + 1) * width] = (acc[:, :width] / acc[:, width:]).astype(BF16)
+        for i in todo[:1]:
+            forward_weight(0, i)
+        todo = todo[1:]
 
     tile = 256
 
@@ -325,15 +333,17 @@
     for rc in (3, 1, 2):
         send(norm_all.at[0, 0], norm_all.at[rc, 0], n_s.at[rc], n_r.at[rc], mate(rc), core)
     send(norm_all.at[0, 0], norm_all.at[0, 1], n_s.at[4], n_r.at[4], sp, 1 - core)
+    for k in [0] + near:
+        send_weight(1, 1, k)
     for i in todo:
         forward_weight(0, i)
-    for i in order[:1] + order[1:5]:
+    for i in order[:4]:
         forward_weight(1, i)
     for rc in (1, 2, 3):
         arrive(norm_all.at[rc, 0], n_s.at[rc], n_r.at[rc])
         j = 4 + rc
         send(norm_all.at[rc, 0], norm_all.at[rc, 1], n_s.at[j], n_r.at[j], sp, 1 - core)
-    for i in order[5:]:
+    for i in order[4:6]:
         forward_weight(1, i)
     last_weight(0)
     for rc in range(4):
@@ -348,9 +358,25 @@
         raised = jnp.dot(tokens, w, preferred_element_type=F32)
         hidden[rc, :, lanes] = jnp.square(jnp.maximum(raised, 0.0)).astype(BF16)
 
+    for i in order[6:]:
+        forward_weight(1, i)
     last_weight(1)
     blocks = tile // depth
 
+    def reduce_pair(rc):
+        arrive(outs_in.at[rc], o_s.at[rc], o_r.at[rc])
+        if rc:
+
+            @pl.loop(0, half // group)
+            def _(t):
+                rws = pl.ds(pl.multiple_of(t * group, group), group)
+                sums[rc - 1, rws] = (
+                    outs[rc, 0, rws].astype(F32) + outs_in[rc, rws].astype(F32)
+                ).astype(BF16)
+
+            send(sums.at[rc - 1], final_in.at[rc - 1], f_s.at[rc], f_r.at[rc], mate(rc), core)
+
+    before = None
     for rc in (3, 1, 2, 0):
 
         @pl.loop(0, model // tile)
@@ -362,19 +388,10 @@
             outs[rc, 1, :, lanes] = o[half:]
 
         send(outs.at[rc, 1], outs_in.at[rc], o_s.at[rc], o_r.at[rc], sp, 1 - core)
-
-    for rc in (3, 1, 2, 0):
-        arrive(outs_in.at[rc], o_s.at[rc], o_r.at[rc])
-        if rc:
-
-            @pl.loop(0, half // group)
-            def _(t):
-                rws = pl.ds(pl.multiple_of(t * group, group), group)
-                sums[rc - 1, rws] = (
-                    outs[rc, 0, rws].astype(F32) + outs_in[rc, rws].astype(F32)
-                ).astype(BF16)
-
-            send(sums.at[rc - 1], final_in.at[rc - 1], f_s.at[rc], f_r.at[rc], mate(rc), core)
+        if before is not None:
+            reduce_pair(before)
+        before = rc
+    reduce_pair(0)
     for rc in (1, 2, 3):
         arrive(final_in.at[rc - 1], f_s.at[rc], f_r.at[rc])
 
@@ -404,18 +421,25 @@
     own_keys = lax.dynamic_index_in_dim(keys, kv_index, 1, keepdims=True)
     own_values = lax.dynamic_index_in_dim(values, kv_index, 1, keepdims=False)
     key_rot = rotate(head_norm(own_keys.astype(F32), key_gain), positions)[:, 0, :].astype(BF16)
-    query_rot = rotate(head_norm(queries.astype(F32), query_gain), positions).astype(BF16)
+    query_rot = rotate(head_norm(queries.astype(F32), query_gain), positions)
+    query_rot = (query_rot * (width ** (-0.5) * LOG2E)).astype(BF16)
+    kinds = jnp.arange(16, dtype=jnp.int32)
+    marks = jnp.where(documents[:, None] == jnp.arange(width)[None, :], APART, 0.0).astype(BF16)
+    marks = jnp.broadcast_to(marks[None], (heads, rows, width))
+    key_rows = jnp.concatenate(
+        [key_rot.T, (kinds[:, None] == documents[None, :]).astype(BF16)], axis=0
+    )
     vm = pl.BlockSpec(memory_space=pltpu.VMEM)
     dma = pltpu.SemaphoreType.DMA
     token = (half, model)
     return pl.pallas_call(
         layer_kernel,
         out_shape=jax.ShapeDtypeStruct(token, BF16),
-        in_specs=[vm] * 9,
+        in_specs=[vm] * 8,
         out_specs=vm,
         scratch_shapes=[
-            pltpu.VMEM((n_sp, 2, rows, width), BF16),
-            pltpu.VMEM((n_sp, 1, rows), jnp.int32),
+            pltpu.VMEM((n_sp, 2 * width, rows), BF16),
+            pltpu.VMEM((n_sp, rows, 2 * width), BF16),
             pltpu.VMEM((rows, heads * width), BF16),
             pltpu.VMEM((n_sp, depth, cols), BF16),
             pltpu.VMEM((n_sp, depth, cols), BF16),
@@ -436,10 +460,9 @@
             collective_id=0, has_side_effects=True, vmem_limit_bytes=60 * 1024 * 1024
         ),
     )(
-        query_rot.transpose(1, 0, 2),
-        jnp.stack([key_rot, own_values]),
-        documents[None, :],
-        documents[:, None],
+        jnp.concatenate([query_rot.transpose(1, 0, 2), marks], axis=-1),
+        key_rows,
+        own_values,
         out_weight,
         residual,
         norm_gain[None, :],

time: 181 us -> 171 us (0.945)
  Pallas kernels: 171 us -> 161 us
    pallas_call x1, Pallas kernels: 171 us -> 161 us  [fused_body(): pl.pallas_call(layer_kernel, out_shape=jax.ShapeDtypeStruct(token, BF16),...]
where the time goes in v2:
time: 171 us
  Pallas kernels  161 us (94%)
  other arithmetic  5.86 us (3%)
  local copies, waits for them, and re-layouts  4.17 us (2%)
    pallas_call x1, Pallas kernels, fused_body(): pl.pallas_call(layer_kernel, out_shape=jax.ShapeDtypeStruct(token, BF16),...  161 us

profile of v2, /device:TPU:0, one launch (start us, length us, event | category | flops | bytes accessed | tf_op | source)
XLA Modules:
  0.0 170.9 jit_solution(5758880054564742174)
XLA Ops:
  0.0 0.0 copy-start
  0.0 0.0 copy-start.2
  0.0 1.3 constant_dynamic-slice_fusion
  1.3 0.1 copy.21
  1.5 0.7 fusion.7
  2.3 0.1 fusion.14
  2.3 0.9 fusion.12
  3.3 0.7 fusion.13
  4.0 0.6 pad_maximum_fusion.3.key_ref
  4.6 0.6 copy.28
  5.2 0.2 fusion.11
  5.5 0.1 copy.17
  5.6 0.1 copy.18
  5.7 0.0 copy-done
  5.7 0.2 fusion
  5.9 0.0 copy-done.2
  5.9 0.2 fusion.1
  6.1 0.5 slice_negate_fusion.1
  6.6 0.0 copy-start.1
  6.6 0.6 fusion.5
  7.2 0.0 copy-done.1
  7.3 0.1 select_convert_fusion
  7.4 0.9 pad_maximum_fusion.q_ref
  8.3 160.8 %shard_map.109 = bf16[128,2048]{1,0:T(8,128)(2,1)} custom-call(bf16[4,256,256]{2,1,0:T(8,128)(2,1)} %pad_maximum_fusion.q_ref, bf16[144,256]{1,0:T(8,128)(2,1)} %pad_maximum_fusion.3.key_ref, bf16[256,128]{1,0:T(8,128)(2,1)} %bitcast.14, bf16[512,2048]{1,0:T(8,128)(2,1)} %ow_ref.1, bf16[256,2048]{1,0:T(8,128)(2,1)} %res_ref.1, f32[1,2048]{1,0:T(1,128)} %bitcast.15, ...), custom_call_target="tpu_custom_call" | custom-call | tf_op jit(solution)/shard_map/pallas_call | solution.py:435
  169.1 1.9 %copy.30 = bf16[128,2048]{1,0:T(8,128)(2,1)} copy(bf16[128,2048]{1,0:T(8,128)(2,1)} %shard_map.109) | data formatting | bytes 1048576
  (7 shorter events, 0.1 us)
Async XLA Ops:
  0.0 5.7 %copy-start = (bf16[256,4,128]{2,1,0:T(4,128)(2,1)S(1)}, bf16[256,4,128]{2,1,0:T(4,128)(2,1)}, u32[]{:S(2)}) copy-start(bf16[256,4,128]{2,1,0:T(4,128)(2,1)} %param.11) | copy-start | bytes 786436
  0.0 5.9 %copy-start.2 = (f32[128]{0:T(128)S(1)}, f32[128]{0:T(128)}, u32[]{:S(2)}) copy-start(f32[128]{0:T(128)} %param.15) | copy-start | bytes 1540
  6.6 0.7 copy-start.1
